TPU v7x, 32 devices: a whole 2x2x4 slice. The times are simulated.
32 devices in a mesh: grp: 2 (over y), sp: 4 (over z), tp: 4 (over x, core).
Axes of the slice: x: 2, y: 2, z: 4, core: 2. Of those that a mesh axis runs over, the one named last changes fastest.
Arguments:
- hidden_in: bfloat16 [3072, 4096], P(('grp', 'sp'), 'tp'), parts along dimension 0, may hold values from -30 to 30
- in_gain: float32 [2, 4096], P(None, 'tp'), may hold values from 0.1 to 1.9
- w_value: bfloat16 [2, 4096, 2048], P(None, 'sp', 'tp'), may hold values from -0.09375 to 0.09375
- w_gate: bfloat16 [2, 4096, 2048], P(None, 'sp', 'tp'), may hold values from -0.09375 to 0.09375
- conv_taps: float32 [2, 31, 2048], P(None, None, 'tp'), may hold values from -9 to 9
- norm_gain: float32 [2, 2048], P(None, 'tp'), may hold values from 0.1 to 1.9
- norm_shift: float32 [2, 2048], P(None, 'tp'), may hold values from -3 to 3
- w_out: bfloat16 [2, 2048, 4096], P(None, 'tp', 'sp'), may hold values from -0.125 to 0.125
Outputs:
- hidden_out: bfloat16 [3072, 4096], P(('grp', 'sp'), 'tp'), parts along dimension 0
There are 2 independent parts, one for each index of `grp`. A program takes and returns all parts, laid end to end along the dimension named above; an argument that names none is the same for every part. Nothing has to cross between parts.
All inputs are finite; a program needn't handle non-finite values.
Results may differ from a plain program's by a relative error of at most 0.013.
Values may be sent and summed in bfloat16 or wider, within the bound.
A program may use at most 64 MiB of HBM per device.

v0:
```python
import jax
import jax.numpy as jnp
from jax import lax
from jax.sharding import PartitionSpec as P

D = 4096
C = 2048
epsilon = 1e-06


def passed_along(value, axis, steps):
    count = lax.axis_size(axis)
    initial, last = (max(0, -steps), min(count, count - steps))
    return lax.ppermute(value, axis, [(source, source + steps) for source in range(initial, last)])


def depthwise(extended, kernel_taps):
    conved = lax.conv_general_dilated(
        extended.astype(jnp.float32)[None],
        kernel_taps[:, None, :],
        (1,),
        [(0, 0)],
        dimension_numbers=("NWC", "WIO", "NWC"),
        feature_group_count=extended.shape[1],
        precision=lax.Precision.HIGHEST,
    )
    return conved[0]


def shards(hidden_in, in_gain, w_value, w_gate, conv_taps, norm_gain, norm_shift, w_out):
    layer_count = w_value.shape[0]
    reach_rows = conv_taps.shape[1] - 1
    value_all, gate_all = (
        lax.all_gather(w_value, "sp", axis=1, tiled=True),
        lax.all_gather(w_gate, "sp", axis=1, tiled=True),
    )
    out_all = lax.all_gather(w_out, "sp", axis=2, tiled=True)
    current = hidden_in
    for layer_idx in range(layer_count):
        widened = current.astype(jnp.float32)
        squares = lax.psum(jnp.sum(widened * widened, axis=1), "tp")
        normalized = (
            widened * lax.rsqrt(squares / D + epsilon)[:, None] * in_gain[layer_idx]
        ).astype(jnp.bfloat16)
        gathered = lax.all_gather(normalized, "tp", axis=1, tiled=True)
        value_part = jnp.dot(gathered, value_all[layer_idx], preferred_element_type=jnp.float32)
        gate_part = jnp.dot(gathered, gate_all[layer_idx], preferred_element_type=jnp.float32)
        gated = (value_part * jax.nn.sigmoid(gate_part)).astype(jnp.bfloat16)
        before = passed_along(gated[gated.shape[0] - reach_rows :], "sp", 1)
        extended = jnp.concatenate([before, gated], axis=0)
        residual = current
        conved = depthwise(extended, conv_taps[layer_idx])
        total_sum, total_squares = lax.psum(
            (jnp.sum(conved, axis=1), jnp.sum(conved * conved, axis=1)), "tp"
        )
        row_mean = total_sum / C
        spread = total_squares / C - row_mean * row_mean
        normed = (conved - row_mean[:, None]) * lax.rsqrt(spread + epsilon)[:, None] * norm_gain[
            layer_idx
        ] + norm_shift[layer_idx]
        mixed_out = jax.nn.silu(normed).astype(jnp.bfloat16)
        partial_value = jnp.dot(mixed_out, out_all[layer_idx], preferred_element_type=jnp.float32)
        summed = lax.psum_scatter(
            partial_value.astype(jnp.bfloat16), "tp", scatter_dimension=1, tiled=True
        ).astype(jnp.float32)
        current = (residual.astype(jnp.float32) + summed).astype(jnp.bfloat16)
    return current


def solution(mesh):
    placed = (
        P(("grp", "sp"), "tp"),
        P(None, "tp"),
        P(None, "sp", "tp"),
        P(None, "sp", "tp"),
        P(None, None, "tp"),
        P(None, "tp"),
        P(None, "tp"),
        P(None, "tp", "sp"),
    )
    return jax.shard_map(
        shards, mesh=mesh, in_specs=placed, out_specs=P(("grp", "sp"), "tp"), check_vma=False
    )
```

profile of v0, /device:TPU:0, one launch (start us, length us, event | category | flops | bytes accessed | tf_op | source)
XLA Modules:
  0.0 657.1 jit_solution(9422213232833642842)
XLA Ops:
  6.5 1.4 fusion.4
  7.9 8.4 %psum.42 = f32[384]{0:T(512)S(1)} all-reduce(f32[384]{0:T(512)S(1)} %fusion.4), channel_id=1, replica_groups=mesh['grp'=2,'sp'=4,'tp'=4] {'tp'}, use_global_device_ids=true, to_apply=%region_1.0 | all-reduce | flops 384 | bytes 3072 | tf_op jit(solution)/shard_map/psum | solution.py:41
  16.3 0.8 fusion.62
  17.1 2.3 fusion.6
  19.3 0.0 all-gather.6.cloned.1.call-update
  19.4 0.0 copy-start.2
  19.4 0.0 all-gather.10.cloned.1.call-start
  19.4 0.7 all-gather.10.cloned.1.call-update
  20.1 0.0 all-gather.8.cloned.1.call-start
  20.2 0.7 all-gather.8.cloned.1.call-update
  20.9 0.0 all-gather.12.cloned.1.call-start
  20.9 0.5 all-gather.12.cloned.1.call-update
  21.4 0.0 reduce-scatter.3.cloned.1.call-start
  21.5 26.8 %all-gather.6.cloned.1.call-done = bf16[384,4096]{1,0:T(8,128)(2,1)} async-done(((bf16[384,1024]{1,0:T(8,128)(2,1)}), bf16[384,4096]{1,0:T(8,128)(2,1)}) %all-gather.6.cloned.1.call-update) | async-done | bytes 3145744 | tf_op jit(solution)/shard_map/all_gather | solution.py:45
  48.3 151.2 %all-gather.10.cloned.1.call-done = bf16[2,4096,512]{2,1,0:T(8,128)(2,1)} async-done(((bf16[2,1024,512]{2,1,0:T(8,128)(2,1)}), bf16[2,4096,512]{2,1,0:T(8,128)(2,1)}) %all-gather.10.cloned.1.call-update) | async-done | bytes 8388624 | tf_op jit(solution)/shard_map/all_gather | solution.py:35
  199.5 5.9 fusion.23
  205.5 143.5 %all-gather.8.cloned.1.call-done = bf16[2,4096,512]{2,1,0:T(8,128)(2,1)} async-done(((bf16[2,1024,512]{2,1,0:T(8,128)(2,1)}), bf16[2,4096,512]{2,1,0:T(8,128)(2,1)}) %all-gather.8.cloned.1.call-update) | async-done | bytes 8388624 | tf_op jit(solution)/shard_map/all_gather | solution.py:34
  349.0 4.2 fusion.25
  353.1 0.0 copy-start.6
  353.2 0.0 copy-start.7
  353.2 1.4 collective-permute-start
  354.6 1.6 collective-permute-done
  356.2 0.1 maximum_bitcast_fusion
  356.3 0.1 reshape.56
  356.4 0.1 copy.14
  356.6 0.1 slice.73
  356.6 1.9 fusion.65
  358.5 0.5 copy.16
  359.0 0.1 reshape.62
  359.1 0.5 copy.15
  359.6 0.1 reshape.60
  359.7 0.2 slice_reduce_fusion.1
  359.9 6.6 all-reduce.1
  366.5 131.7 %all-gather.12.cloned.1.call-done = bf16[2,512,4096]{2,1,0:T(8,128)(2,1)} async-done(((bf16[2,512,1024]{2,1,0:T(8,128)(2,1)}), bf16[2,512,4096]{2,1,0:T(8,128)(2,1)}) %all-gather.12.cloned.1.call-update) | async-done | bytes 8388624 | tf_op jit(solution)/shard_map/all_gather | solution.py:37
  498.2 5.9 convolution_convert_fusion.1
  504.1 0.0 reduce-scatter.3.cloned.1.call-update
  504.1 0.0 all-gather.14.cloned.1.call-start
  504.2 36.0 %reduce-scatter.3.cloned.1.call-done = bf16[384,1024]{1,0:T(8,128)(2,1)} async-done(((bf16[384,4096]{1,0:T(8,128)(2,1)}), bf16[384,1024]{1,0:T(8,128)(2,1)}) %reduce-scatter.3.cloned.1.call-update) | async-done | bytes 786448 | tf_op jit(solution)/shard_map/reduce_scatter | solution.py:63
  540.2 1.5 fusion.8
  541.6 5.8 psum.45
  547.4 2.3 fusion.10
  549.7 0.0 all-gather.14.cloned.1.call-update
  549.8 0.2 reduce-scatter.5.cloned.1.call-start
  550.0 29.1 %all-gather.14.cloned.1.call-done = bf16[384,4096]{1,0:T(8,128)(2,1)} async-done(((bf16[384,1024]{1,0:T(8,128)(2,1)}), bf16[384,4096]{1,0:T(8,128)(2,1)}) %all-gather.14.cloned.1.call-update) | async-done | bytes 3145744 | tf_op jit(solution)/shard_map/all_gather | solution.py:45
  579.0 5.2 fusion.21
  584.2 4.0 fusion.24
  588.3 3.4 collective-permute-start.1
  591.7 1.6 collective-permute-done.1
  593.3 0.1 maximum_bitcast_fusion.1
  593.4 0.1 reshape.65
  593.5 0.1 copy.18
  593.6 0.1 slice.80
  593.7 2.0 fusion.66
  595.7 0.5 copy.20
  596.2 0.1 reshape.71
  596.3 0.1 slice_reduce_fusion
  596.5 0.5 copy.19
  597.0 0.1 reshape.69
  597.1 0.1 slice_reduce_fusion.2
  597.2 5.9 all-reduce
  603.2 5.9 convolution_convert_fusion
  609.1 0.0 reduce-scatter.5.cloned.1.call-update
  609.1 38.7 %reduce-scatter.5.cloned.1.call-done = bf16[384,1024]{1,0:T(8,128)(2,1)} async-done(((bf16[384,4096]{1,0:T(8,128)(2,1)}), bf16[384,1024]{1,0:T(8,128)(2,1)}) %reduce-scatter.5.cloned.1.call-update) | async-done | bytes 786448 | tf_op jit(solution)/shard_map/reduce_scatter | solution.py:63
  647.8 2.4 fusion.11
  (24 shorter events, 0.2 us)
Async XLA Ops:
  6.5 41.8 %all-gather.6.cloned.1.call-start = ((), (), s32[]{:S(2)}) async-start(), calls=%async_computation.2 | async-start | bytes 3932160 | tf_op jit(solution)/shard_map/all_gather | solution.py:45
  19.4 2.1 copy-start.2
  19.4 180.2 %all-gather.10.cloned.1.call-start = ((), (), s32[]{:S(2)}) async-start(), calls=%async_computation.4 | async-start | bytes 10485760 | tf_op jit(solution)/shard_map/all_gather | solution.py:35
  20.1 328.8 %all-gather.8.cloned.1.call-start = ((), (), s32[]{:S(2)}) async-start(), calls=%async_computation.3 | async-start | bytes 10485760 | tf_op jit(solution)/shard_map/all_gather | solution.py:34
  20.9 477.4 %all-gather.12.cloned.1.call-start = ((), (), s32[]{:S(2)}) async-start(), calls=%async_computation.5 | async-start | bytes 10485760 | tf_op jit(solution)/shard_map/all_gather | solution.py:37
  21.4 518.8 %reduce-scatter.3.cloned.1.call-start = ((), (), s32[]{:S(2)}) async-start(), calls=%async_computation.6 | async-start | bytes 3932160 | tf_op jit(solution)/shard_map/reduce_scatter | solution.py:63
  48.3 300.6 %copy-start.4 = (bf16[384,4096]{1,0:T(8,128)(2,1)S(1)}, bf16[384,4096]{1,0:T(8,128)(2,1)}, u32[]{:S(2)}) copy-start(bf16[384,4096]{1,0:T(8,128)(2,1)} %all-gather.6.cloned.1.call-done) | copy-start | bytes 9437188
  205.5 149.1 %copy-start.3 = (f32[2,512]{1,0:T(2,128)S(1)}, f32[2,512]{1,0:T(2,128)}, u32[]{:S(2)}) copy-start(f32[2,512]{1,0:T(2,128)} %param.14) | copy-start | bytes 12292
  353.1 3.5 copy-start.6
  353.2 3.5 copy-start.7
  353.2 3.0 collective-permute-start
  504.1 36.1 %copy-start = (bf16[384,1024]{1,0:T(8,128)(2,1)S(1)}, bf16[384,1024]{1,0:T(8,128)(2,1)}, u32[]{:S(2)}) copy-start(bf16[384,1024]{1,0:T(8,128)(2,1)} %param.8) | copy-start | bytes 2359300
  504.1 74.9 %all-gather.14.cloned.1.call-start = ((), (), s32[]{:S(2)}) async-start(), calls=%async_computation.7 | async-start | bytes 3932160 | tf_op jit(solution)/shard_map/all_gather | solution.py:45
  549.8 98.0 %reduce-scatter.5.cloned.1.call-start = ((), (), s32[]{:S(2)}) async-start(), calls=%async_computation.8 | async-start | bytes 3932160 | tf_op jit(solution)/shard_map/reduce_scatter | solution.py:63
  579.0 5.2 copy-start.5
  588.3 5.0 collective-permute-start.1
  609.1 38.7 %copy-start.1 = (bf16[384,1024]{1,0:T(8,128)(2,1)S(1)}, bf16[384,1024]{1,0:T(8,128)(2,1)}, u32[]{:S(2)}) copy-start(bf16[384,1024]{1,0:T(8,128)(2,1)} %reduce-scatter.3.cloned.1.call-done) | copy-start | bytes 2359300
Sparse Core Ops, SparseCore 0:
  19.5 28.8 all-gather.5
  49.9 149.6 all-gather.9
  201.1 147.7 all-gather.7
  350.4 147.7 all-gather.11
  504.2 35.8 reduce-scatter.2
  549.9 29.1 all-gather.13
  609.2 38.5 reduce-scatter.4
where the time goes:
time: 658 us; the launch traced here: 657 us
  waiting for transfers between devices  562 us (85%)
  matrix products  35 us (5%)
  blocking collectives  26.6 us (4%)
  between operations  13.8 us (2%)
  other arithmetic  10.6 us (2%)
    all_gather x1, waiting for transfers between devices, shards(): lax.all_gather(w_gate, 'sp', axis=1, tiled=True)  151 us
    all_gather x1, waiting for transfers between devices, shards(): lax.all_gather(w_value, 'sp', axis=1, tiled=True)  143 us
    all_gather x1, waiting for transfers between devices, shards(): out_all = lax.all_gather(w_out, 'sp', axis=2, tiled=True)  132 us
    reduce_scatter x2, waiting for transfers between devices, shards(): lax.psum_scatter(partial_value.astype(jnp.bfloat16), 'tp', scatter_dimens...  74.7 us
    all_gather x2, waiting for transfers between devices, shards(): gathered = lax.all_gather(normalized, 'tp', axis=1, tiled=True)  55.9 us
    psum x2, blocking collectives, shards(): squares = lax.psum(jnp.sum(widened * widened, axis=1), 'tp')  14.1 us
  transfers between devices with their start and end apart: 9, of which 9 were waited for; matrix products, arithmetic and copies ran while one was open for 2% of the time, Pallas kernels for 0%

commit v1 on v0

--- a/solution.py
+++ b/solution.py
@@ -34,7 +34,12 @@
         lax.all_gather(w_value, "sp", axis=1, tiled=True),
         lax.all_gather(w_gate, "sp", axis=1, tiled=True),
     )
-    out_all = lax.all_gather(w_out, "sp", axis=2, tiled=True)
+    ring = [w_out]
+    for hop in range(3):
+        ring.append(lax.ppermute(ring[-1], "sp", [(dev, (dev + 1) % 4) for dev in range(4)]))
+    out_all = jnp.roll(
+        jnp.concatenate(ring[::-1], axis=2), (lax.axis_index("sp") + 1) * ring[0].shape[2], axis=2
+    )
     current = hidden_in
     for layer_idx in range(layer_count):
         widened = current.astype(jnp.float32)

time: 658 us -> 611 us (0.929)
  waiting for transfers between devices: 562 us -> 433 us
  starting transfers between devices: 5.24 us -> 67.2 us
  local copies, waits for them, and re-layouts: 3.79 us -> 23.5 us
    ppermute x0 -> x3, waiting for transfers between devices: none -> 216 us  [shards(): lax.ppermute(ring[-1], 'sp', [(dev, (dev + 1) % 4) for dev in range(4)])]
    all_gather x1, waiting for transfers between devices: 151 us -> 0.01 us  [shards(): lax.all_gather(w_gate, 'sp', axis=1, tiled=True)]
    all_gather x1 -> x0, waiting for transfers between devices: 132 us -> none  [shards(): out_all = lax.all_gather(w_out, 'sp', axis=2, tiled=True)]
    ppermute x0 -> x3, starting transfers between devices: none -> 61.8 us  [shards(): lax.ppermute(ring[-1], 'sp', [(dev, (dev + 1) % 4) for dev in range(4)])]
    all_gather x1, waiting for transfers between devices: 143 us -> 108 us  [shards(): lax.all_gather(w_value, 'sp', axis=1, tiled=True)]
    all_gather x2, waiting for transfers between devices: 55.9 us -> 29.1 us  [shards(): gathered = lax.all_gather(normalized, 'tp', axis=1, tiled=True)]
    unnamed x16 -> x27, local copies, waits for them, and re-layouts: 0.04 us -> 18.3 us
  transfers between devices with their start and end apart: 9 -> 11, of which waited for: 9 -> 9; matrix products, arithmetic and copies ran while one was open for 2% -> 4% of each run, Pallas kernels for 0% -> 0%
where the time goes in v1:
time: 611 us; the launch traced here: 610 us
  waiting for transfers between devices  433 us (71%)
  starting transfers between devices  67.2 us (11%)
  matrix products  34.8 us (6%)
  blocking collectives  26.6 us (4%)
  local copies, waits for them, and re-layouts  23.5 us (4%)
  between operations  13.8 us (2%)
  other arithmetic  10.8 us (2%)
    ppermute x3, waiting for transfers between devices, shards(): lax.ppermute(ring[-1], 'sp', [(dev, (dev + 1) % 4) for dev in range(4)])  216 us
    all_gather x1, waiting for transfers between devices, shards(): lax.all_gather(w_value, 'sp', axis=1, tiled=True)  108 us
    reduce_scatter x2, waiting for transfers between devices, shards(): lax.psum_scatter(partial_value.astype(jnp.bfloat16), 'tp', scatter_dimens...  77.6 us
    ppermute x3, starting transfers between devices, shards(): lax.ppermute(ring[-1], 'sp', [(dev, (dev + 1) % 4) for dev in range(4)])  61.8 us
    all_gather x2, waiting for transfers between devices, shards(): gathered = lax.all_gather(normalized, 'tp', axis=1, tiled=True)  29.1 us
    unnamed x27, local copies, waits for them, and re-layouts  18.3 us
    psum x2, blocking collectives, shards(): squares = lax.psum(jnp.sum(widened * widened, axis=1), 'tp')  14.1 us
    psum x2, blocking collectives, shards(): lax.psum((jnp.sum(conved, axis=1), jnp.sum(conved * conved, axis=1)), 'tp')  12.5 us
  transfers between devices with their start and end apart: 11, of which 9 were waited for; matrix products, arithmetic and copies ran while one was open for 4% of the time, Pallas kernels for 0%

profile of v1, /device:TPU:0, one launch (start us, length us, event | category | flops | bytes accessed | tf_op | source)
XLA Modules:
  0.0 609.8 jit_solution(9408921119890468791)
XLA Ops:
  6.5 0.8 fusion.64
  7.3 1.4 fusion.4
  8.7 8.4 %psum.42 = f32[384]{0:T(512)S(1)} all-reduce(f32[384]{0:T(512)S(1)} %fusion.4), channel_id=1, replica_groups=mesh['grp'=2,'sp'=4,'tp'=4] {'tp'}, use_global_device_ids=true, to_apply=%region_1.2 | all-reduce | flops 384 | bytes 3072 | tf_op jit(solution)/shard_map/psum | solution.py:46
  17.1 2.4 fusion.6
  19.6 0.7 all-gather.9.cloned.1.call-update
  20.3 0.7 all-gather.7.cloned.1.call-update
  21.1 1.6 collective-permute-start.1
  22.7 53.8 %collective-permute-done.1 = bf16[2,512,1024]{2,1,0:T(8,128)(2,1)S(1)} collective-permute-done((bf16[2,512,1024]{2,1,0:T(8,128)(2,1)S(1)}, bf16[2,512,1024]{2,1,0:T(8,128)(2,1)S(1)}, u32[]{:S(2)}, u32[]{:S(2)}) %collective-permute-start.1) | collective-permute-done | bytes 2097184 | tf_op jit(solution)/shard_map/ppermute | solution.py:39
  76.5 1.3 copy-done.2
  77.9 9.7 %collective-permute-start.2 = (bf16[2,512,1024]{2,1,0:T(8,128)(2,1)S(1)}, bf16[2,512,1024]{2,1,0:T(8,128)(2,1)}, u32[]{:S(2)}, u32[]{:S(2)}) collective-permute-start(bf16[2,512,1024]{2,1,0:T(8,128)(2,1)S(1)} %collective-permute-done.1), channel_id=1, source_target_pairs={{0,4},{4,8},{8,12},{12,0},{1,5},{5,9},{9,13},{13,1},{2,6},{6,10},{... | collective-permute-start | bytes 6291464 | tf_op jit(solution)/shard_map/ppermute | solution.py:39
  87.6 89.0 %collective-permute-done.2 = bf16[2,512,1024]{2,1,0:T(8,128)(2,1)} collective-permute-done((bf16[2,512,1024]{2,1,0:T(8,128)(2,1)S(1)}, bf16[2,512,1024]{2,1,0:T(8,128)(2,1)}, u32[]{:S(2)}, u32[]{:S(2)}) %collective-permute-start.2) | collective-permute-done | bytes 2097184 | tf_op jit(solution)/shard_map/ppermute | solution.py:39
  176.6 50.4 %collective-permute-start.3 = (bf16[2,512,1024]{2,1,0:T(8,128)(2,1)}, bf16[2,512,1024]{2,1,0:T(8,128)(2,1)}, u32[]{:S(2)}, u32[]{:S(2)}) collective-permute-start(bf16[2,512,1024]{2,1,0:T(8,128)(2,1)} %collective-permute-done.2), channel_id=1, source_target_pairs={{0,4},{4,8},{8,12},{12,0},{1,5},{5,9},{9,13},{13,1},{2,6},{6,10},{... | collective-permute-start | bytes 6291464 | tf_op jit(solution)/shard_map/ppermute | solution.py:39
  227.1 72.8 %collective-permute-done.3 = bf16[2,512,1024]{2,1,0:T(8,128)(2,1)} collective-permute-done((bf16[2,512,1024]{2,1,0:T(8,128)(2,1)}, bf16[2,512,1024]{2,1,0:T(8,128)(2,1)}, u32[]{:S(2)}, u32[]{:S(2)}) %collective-permute-start.3) | collective-permute-done | bytes 2097184 | tf_op jit(solution)/shard_map/ppermute | solution.py:39
  299.9 3.1 constant_dynamic-update-slice_fusion.7
  303.0 3.1 constant_dynamic-update-slice_fusion.6
  306.1 1.5 constant_dynamic-update-slice_fusion.5
  307.6 1.5 constant_dynamic-update-slice_fusion.4
  309.1 3.1 constant_dynamic-update-slice_fusion.3
  312.2 3.1 constant_dynamic-update-slice_fusion.2
  315.3 1.5 constant_dynamic-update-slice_fusion.1
  316.8 5.1 fusion.23
  321.9 107.8 %all-gather.7.cloned.1.call-done = bf16[2,4096,512]{2,1,0:T(8,128)(2,1)} async-done(((bf16[2,1024,512]{2,1,0:T(8,128)(2,1)}), bf16[2,4096,512]{2,1,0:T(8,128)(2,1)}) %all-gather.7.cloned.1.call-update) | async-done | bytes 8388624 | tf_op jit(solution)/shard_map/all_gather | solution.py:34
  429.7 4.9 fusion.25
  434.7 1.7 collective-permute-start
  436.4 1.5 constant_dynamic-update-slice_fusion
  437.9 0.1 collective-permute-done
  438.0 0.1 maximum_bitcast_fusion
  438.1 0.1 reshape.56
  438.2 0.1 copy.14
  438.3 0.1 slice.73
  438.4 1.9 fusion.67
  440.3 0.5 copy.15
  440.8 0.1 reshape.60
  440.9 0.5 copy.16
  441.4 0.1 reshape.62
  441.5 0.2 slice_reduce_fusion.1
  441.7 6.5 %all-reduce.1 = (f32[384]{0:T(512)S(1)}, f32[384]{0:T(512)S(1)}) all-reduce(f32[384]{0:T(512)S(1)} %get-tuple-element.23, f32[384]{0:T(512)S(1)} %get-tuple-element.24), channel_id=1, replica_groups=mesh['grp'=2,'sp'=4,'tp'=4] {'tp'}, use_global_device_ids=true, to_apply=%region_5.6 | all-reduce | flops 768 | bytes 6144 | tf_op jit(solution)/shard_map/psum | solution.py:58
  448.2 5.8 convolution_convert_fusion.1
  454.1 0.0 all-gather.11.cloned.1.call-start
  454.1 38.9 %reduce-scatter.3.cloned.1.call-done = bf16[384,1024]{1,0:T(8,128)(2,1)} async-done(((bf16[384,4096]{1,0:T(8,128)(2,1)}), bf16[384,1024]{1,0:T(8,128)(2,1)}) %reduce-scatter.3.cloned.1.call-update) | async-done | bytes 786448 | tf_op jit(solution)/shard_map/reduce_scatter | solution.py:68
  493.0 1.5 fusion.8
  494.5 5.8 psum.45
  500.2 2.3 fusion.10
  502.6 0.2 reduce-scatter.5.cloned.1.call-start
  502.8 29.1 %all-gather.11.cloned.1.call-done = bf16[384,4096]{1,0:T(8,128)(2,1)} async-done(((bf16[384,1024]{1,0:T(8,128)(2,1)}), bf16[384,4096]{1,0:T(8,128)(2,1)}) %all-gather.11.cloned.1.call-update) | async-done | bytes 3145744 | tf_op jit(solution)/shard_map/all_gather | solution.py:50
  531.9 5.2 fusion.21
  537.1 4.0 fusion.24
  541.1 3.4 collective-permute-start.4
  544.5 1.6 collective-permute-done.4
  546.0 0.1 maximum_bitcast_fusion.1
  546.2 0.1 reshape.65
  546.3 0.1 copy.18
  546.4 0.1 slice.79
  546.5 2.1 fusion.68
  548.5 0.5 copy.19
  549.0 0.1 reshape.69
  549.1 0.5 copy.20
  549.6 0.1 reshape.71
  549.7 0.1 slice_reduce_fusion
  549.9 0.2 slice_reduce_fusion.2
  550.0 5.9 all-reduce
  556.0 5.8 convolution_convert_fusion
  561.8 38.7 %reduce-scatter.5.cloned.1.call-done = bf16[384,1024]{1,0:T(8,128)(2,1)} async-done(((bf16[384,4096]{1,0:T(8,128)(2,1)}), bf16[384,1024]{1,0:T(8,128)(2,1)}) %reduce-scatter.5.cloned.1.call-update) | async-done | bytes 786448 | tf_op jit(solution)/shard_map/reduce_scatter | solution.py:68
  600.6 2.4 fusion.11
  (39 shorter events, 0.4 us)
Async XLA Ops:
  6.5 310.2 %all-gather.5.cloned.1.call-start = ((), (), s32[]{:S(2)}) async-start(), calls=%async_computation.2 | async-start | bytes 3932160 | tf_op jit(solution)/shard_map/all_gather | solution.py:50
  17.1 4.0 copy-start.1
  17.1 210.0 %copy-start.5 = (f32[2,512]{1,0:T(2,128)S(1)}, f32[2,512]{1,0:T(2,128)}, u32[]{:S(2)}) copy-start(f32[2,512]{1,0:T(2,128)} %param.14) | copy-start | bytes 12292
  17.1 210.0 %copy-start.6 = (f32[2,512]{1,0:T(2,128)S(1)}, f32[2,512]{1,0:T(2,128)}, u32[]{:S(2)}) copy-start(f32[2,512]{1,0:T(2,128)} %param.13) | copy-start | bytes 12292
  19.5 297.3 %all-gather.9.cloned.1.call-start = ((), (), s32[]{:S(2)}) async-start(), calls=%async_computation.4 | async-start | bytes 10485760 | tf_op jit(solution)/shard_map/all_gather | solution.py:35
  20.3 409.4 %all-gather.7.cloned.1.call-start = ((), (), s32[]{:S(2)}) async-start(), calls=%async_computation.3 | async-start | bytes 10485760 | tf_op jit(solution)/shard_map/all_gather | solution.py:34
  21.0 472.0 %reduce-scatter.3.cloned.1.call-start = ((), (), s32[]{:S(2)}) async-start(), calls=%async_computation.5 | async-start | bytes 3932160 | tf_op jit(solution)/shard_map/reduce_scatter | solution.py:68
  21.1 55.5 %collective-permute-start.1 = (bf16[2,512,1024]{2,1,0:T(8,128)(2,1)S(1)}, bf16[2,512,1024]{2,1,0:T(8,128)(2,1)S(1)}, u32[]{:S(2)}, u32[]{:S(2)}) collective-permute-start(bf16[2,512,1024]{2,1,0:T(8,128)(2,1)S(1)} %copy-done.1), channel_id=1, source_target_pairs={{0,4},{4,8},{8,12},{12,0},{1,5},{5,9},{9,13},{13,1},{2,6},{6,10},{... | collective-permute-start | bytes 6291464 | tf_op jit(solution)/shard_map/ppermute | solution.py:39
  76.5 1.3 copy-start.2
  77.9 98.7 %collective-permute-start.2 = (bf16[2,512,1024]{2,1,0:T(8,128)(2,1)S(1)}, bf16[2,512,1024]{2,1,0:T(8,128)(2,1)}, u32[]{:S(2)}, u32[]{:S(2)}) collective-permute-start(bf16[2,512,1024]{2,1,0:T(8,128)(2,1)S(1)} %collective-permute-done.1), channel_id=1, source_target_pairs={{0,4},{4,8},{8,12},{12,0},{1,5},{5,9},{9,13},{13,1},{2,6},{6,10},{... | collective-permute-start | bytes 6291464 | tf_op jit(solution)/shard_map/ppermute | solution.py:39
  176.6 123.3 %collective-permute-start.3 = (bf16[2,512,1024]{2,1,0:T(8,128)(2,1)}, bf16[2,512,1024]{2,1,0:T(8,128)(2,1)}, u32[]{:S(2)}, u32[]{:S(2)}) collective-permute-start(bf16[2,512,1024]{2,1,0:T(8,128)(2,1)} %collective-permute-done.2), channel_id=1, source_target_pairs={{0,4},{4,8},{8,12},{12,0},{1,5},{5,9},{9,13},{13,1},{2,6},{6,10},{... | collective-permute-start | bytes 6291464 | tf_op jit(solution)/shard_map/ppermute | solution.py:39
  227.1 79.1 %copy-start.3 = (bf16[2,512,1024]{2,1,0:T(8,128)(2,1)S(1)}, bf16[2,512,1024]{2,1,0:T(8,128)(2,1)}, u32[]{:S(2)}) copy-start(bf16[2,512,1024]{2,1,0:T(8,128)(2,1)} %copy-done.2) | copy-start | bytes 6291460
  434.7 3.7 copy-start.8
  434.7 3.7 copy-start.9
  434.7 3.3 collective-permute-start
  454.0 38.9 %copy-start = (bf16[384,1024]{1,0:T(8,128)(2,1)S(1)}, bf16[384,1024]{1,0:T(8,128)(2,1)}, u32[]{:S(2)}) copy-start(bf16[384,1024]{1,0:T(8,128)(2,1)} %param.8) | copy-start | bytes 2359300
  454.1 77.8 %all-gather.11.cloned.1.call-start = ((), (), s32[]{:S(2)}) async-start(), calls=%async_computation.6 | async-start | bytes 3932160 | tf_op jit(solution)/shard_map/all_gather | solution.py:50
  502.6 98.0 %reduce-scatter.5.cloned.1.call-start = ((), (), s32[]{:S(2)}) async-start(), calls=%async_computation.7 | async-start | bytes 3932160 | tf_op jit(solution)/shard_map/reduce_scatter | solution.py:68
  531.9 5.2 copy-start.7
  541.1 5.0 collective-permute-start.4
  561.8 38.7 %copy-start.4 = (bf16[384,1024]{1,0:T(8,128)(2,1)S(1)}, bf16[384,1024]{1,0:T(8,128)(2,1)}, u32[]{:S(2)}) copy-start(bf16[384,1024]{1,0:T(8,128)(2,1)} %reduce-scatter.3.cloned.1.call-done) | copy-start | bytes 2359300
Sparse Core Ops, SparseCore 0:
  19.6 28.8 all-gather.4
  50.1 226.9 all-gather.8
  278.7 151.0 all-gather.6
  454.2 38.7 reduce-scatter.2
  502.7 29.1 all-gather.10
  562.0 38.5 reduce-scatter.4
